TPU v7x, 32 devices: a whole 2x2x4 slice. The times are simulated.
32 devices in a mesh: sp: 4 (over x, core), dp: 8 (over z, y).
Axes of the slice: x: 2, y: 2, z: 4, core: 2. Of those that a mesh axis runs over, the one named last changes fastest.
Arguments:
- cotangent: bfloat16 [8, 512, 2048], P('dp', 'sp'), may hold values from -6 to 6
- layer_input: bfloat16 [8, 512, 2048], P('dp', 'sp'), may hold values from -6 to 6
- x_pre: bfloat16 [8, 512, 2048], P('dp', None, 'sp'), may hold values from -6 to 6
- z_pre: bfloat16 [8, 512, 2048], P('dp', None, 'sp'), may hold values from -6 to 6
- b_pre: bfloat16 [8, 512, 256], P('dp'), may hold values from -6 to 6
- c_pre: bfloat16 [8, 512, 256], P('dp'), may hold values from -6 to 6
- dt_raw: bfloat16 [8, 512, 32], P('dp', None, 'sp'), may hold values from -4.4 to 11.4
- conv_x: bfloat16 [4, 2048], P(None, 'sp'), may hold values from -3 to 3
- conv_b: bfloat16 [4, 256], replicated, may hold values from -3 to 3
- conv_c: bfloat16 [4, 256], replicated, may hold values from -3 to 3
- dt_bias: float32 [32], P('sp'), may hold values from -3.8 to -3.2
- a_log: float32 [32], P('sp'), may hold values from -9 to 0.5
- d_skip: float32 [32], P('sp'), may hold values from 0.5 to 1.5
- norm_w: float32 [2048], P('sp'), may hold values from 0.1 to 1.9
Outputs:
- d_x_pre: bfloat16 [8, 512, 2048], P('dp', 'sp')
- d_z_pre: bfloat16 [8, 512, 2048], P('dp', 'sp')
- d_b_pre: bfloat16 [8, 512, 256], P('dp', 'sp')
- d_c_pre: bfloat16 [8, 512, 256], P('dp', 'sp')
- d_dt_raw: bfloat16 [8, 512, 32], P('dp', 'sp')
- grad_a_log: float32 [32], P('sp')
- grad_w_dt: float32 [2048, 32], replicated
All inputs are finite; a program needn't handle non-finite values.
Results may differ from a plain program's by a relative error of at most 0.017.
Values may be sent and summed in bfloat16 or wider, within the bound.
A program may use at most 128 MiB of HBM per device.

v0:
```python
import functools

import jax
import jax.numpy as jnp
from jax import lax
from jax.experimental import pallas as pl
from jax.experimental.pallas import tpu as pltpu
from jax.sharding import PartitionSpec as P

GROUPS = 2
STATE = 128
BLOCK = 128
LANES = 128
EPS = 1e-05
MESH = pl.DeviceIdType.MESH
F32 = jnp.float32
BF16 = jnp.bfloat16


def dot(a, b, dims=((1,), (0,)), precision=None):
    return lax.dot_general(a, b, (dims, ((), ())), precision=precision, preferred_element_type=F32)


def split(v):
    hi = v.astype(BF16)
    return hi, (v - hi.astype(F32)).astype(BF16)


def dot3(a, b, dims=((1,), (0,))):
    left = jnp.concatenate([a[0], a[1], a[0]], axis=dims[0][0])
    right = jnp.concatenate([b[0], b[0], b[1]], axis=dims[1][0])
    return dot(left, right, dims)


def iota(axis, shape=(BLOCK, LANES)):
    return lax.broadcasted_iota(jnp.int32, shape, axis)


def silu_parts(u):
    sig = jax.nn.sigmoid(u)
    return u * sig, sig * (1.0 + u * (1.0 - sig))


def mixer_kernel(
    n_sp,
    group_span,
    head_dim,
    heads,
    cot_ref,
    x_ref,
    z_ref,
    b_ref,
    c_ref,
    dt_ref,
    tapx_ref,
    tapb_ref,
    tapc_ref,
    hp_ref,
    cp_ref,
    dx_ref,
    oz_ref,
    db_ref,
    dc_ref,
    dd_ref,
    ga_ref,
    dz_ref,
    z_send,
    z_recv,
    gx_s,
    xa_s,
    xd_s,
    dtp_s,
    ea_s,
    te_s,
    m_s,
    l_s,
    dy_s,
    r_s,
    du_s,
    sin_s,
    st_s,
    bs_s,
    cs_s,
    gb_s,
    gc_s,
    dbu_s,
    dcu_s,
    cum_s,
    step_s,
    dts_s,
    sc_s,
):
    highest = lax.Precision.HIGHEST
    length, channels = x_ref.shape
    tokens = oz_ref.shape[0]
    sp = lax.axis_index("sp")
    peers = [(lax.rem(sp + o, n_sp), o) for o in range(1, n_sp)]
    barrier = pltpu.get_barrier_semaphore()
    for peer, _ in peers:
        pl.semaphore_signal(barrier, inc=1, device_id={"sp": peer}, device_id_type=MESH)
    chunks = length // BLOCK
    pairs = channels // LANES
    group = lax.axis_index("sp") // group_span
    gcol = pl.multiple_of(group * STATE, STATE)
    lane = iota(1)
    row = iota(0)
    per = LANES // head_dim
    half = [(lane // head_dim == k) for k in range(per)]
    causal = row >= lane
    tri = causal.astype(F32)
    triu = (row <= lane).astype(F32)
    same = jnp.where(row // head_dim == lane // head_dim, 1.0 / head_dim, 0.0).astype(BF16)
    bias = hp_ref[0:1, :]
    decay = jnp.exp(hp_ref[1:2, :])
    valid = lax.broadcasted_iota(jnp.int32, (1, LANES), 1) < heads

    same2 = jnp.concatenate([same, same], axis=0)

    def summed(v, ones):
        return dot(jnp.concatenate(split(v), axis=1), ones)

    def conv(ref, taps, c, cols):
        base = pl.multiple_of(c * BLOCK, BLOCK)
        before = pl.multiple_of(jnp.maximum(base - 16, 0), 16)
        head = ref[pl.ds(before, 16), cols].astype(F32)
        head = jnp.where(c > 0, head, 0.0)
        body = ref[pl.ds(base, BLOCK), cols].astype(F32)
        full = jnp.concatenate([head, body], axis=0)
        n = taps.shape[0]
        out = body * taps[n - 1 : n]
        for k in range(n - 1):
            start = 16 - (n - 1 - k)
            out = out + full[start : start + BLOCK] * taps[k : k + 1]
        return out

    def conv_back(body, after, taps, cols):
        full = jnp.concatenate([body, after[:, cols]], axis=0)
        after[:, cols] = body[:8]
        n = taps.shape[0]
        out = full[:BLOCK] * taps[n - 1 : n]
        for k in range(n - 1):
            out = out + full[n - 1 - k : n - 1 - k + BLOCK] * taps[k : k + 1]
        return out

    def pick(parts):
        out = parts[-1]
        for k in range(per - 1):
            out = jnp.where(half[k], parts[k], out)
        return out

    st_s[...] = jnp.zeros_like(st_s)

    def forward(c, carry):
        base = pl.multiple_of(c * BLOCK, BLOCK)
        rows = pl.ds(base, BLOCK)
        ba, gb = silu_parts(conv(b_ref, tapb_ref[:, pl.ds(gcol, STATE)].astype(F32), c, pl.ds(gcol, STATE)))
        ca, gc = silu_parts(conv(c_ref, tapc_ref[:, pl.ds(gcol, STATE)].astype(F32), c, pl.ds(gcol, STATE)))
        gb_s[rows, :] = gb
        gc_s[rows, :] = gc
        bb = split(ba)
        cb = split(ca)
        bs_s[rows, :] = ba
        cs_s[rows, :] = ca
        scores = dot3(cb, bb, ((1,), (1,)))
        pre = dt_ref[rows, :].astype(F32) + bias
        dt = jnp.where(valid, jnp.maximum(pre, 0.0) + jnp.log1p(jnp.exp(-jnp.abs(pre))), 0.0)
        step = -dt * decay
        cum = dot(tri, step, precision=highest)
        dts_s[rows, :] = jax.nn.sigmoid(pre)
        step_s[rows, :] = step
        cum_t = cum.T
        bt = split(ba.T)
        for j in range(pairs):
            cols = pl.ds(j * LANES, LANES)
            xa, gx = silu_parts(conv(x_ref, tapx_ref[:, cols].astype(F32), c, cols))
            gx_s[rows, cols] = gx
            xa_s[rows, cols] = xa
            acols = []
            dcols = []
            ms = []
            for k in range(per):
                h = j * per + k
                acol = jnp.broadcast_to(cum[:, h : h + 1], (BLOCK, LANES))
                acols.append(acol)
                dcols.append(jnp.broadcast_to(dt[:, h : h + 1], (BLOCK, LANES)))
                lam = jnp.exp(jnp.where(causal, acol - cum_t[h : h + 1, :], -jnp.inf))
                m = scores * lam
                ms.append(m)
                m_s[j, pl.ds(c * per * BLOCK + k * BLOCK, BLOCK), :] = m
                l_s[j, pl.ds(c * per * BLOCK + k * BLOCK, BLOCK), :] = lam
            ap = pick(acols)
            dtp = pick(dcols)
            dtp_s[rows, cols] = dtp
            ea = jnp.exp(ap)
            te = jnp.exp(ap[BLOCK - 1 : BLOCK, :] - ap)
            ea_s[rows, cols] = ea
            te_s[rows, cols] = te
            xd = xa * dtp
            xd_s[rows, cols] = xd
            xcat = jnp.concatenate([jnp.where(half[k], xd, 0.0) for k in range(per)], axis=0)
            y = dot3(split(jnp.concatenate(ms, axis=1)), split(xcat))
            st = st_s[:, cols]
            sin_s[pl.ds(c * STATE, STATE), cols] = st
            y = y + dot3(cb, split(st)) * ea
            st_s[:, cols] = st * ea[BLOCK - 1 : BLOCK, :] + dot3(bt, split(xd * te))
            full = y + cp_ref[1:2, cols] * xa
            sz, gz = silu_parts(z_ref[rows, cols].astype(F32))
            gated = full * sz
            inv = lax.rsqrt(summed(gated * gated, same2) + EPS)
            gh = gated * inv
            g = cot_ref[rows, cols].astype(F32) * cp_ref[0:1, cols]
            mean = summed(g * gh, same2)
            dgated = inv * (g - gh * mean)
            dy = dgated * sz
            dz_ref[rows, cols] = (dgated * full * gz).astype(BF16)
            dy_s[rows, cols] = dy
            r_s[rows, cols] = dy * y
        cum_s[rows, :] = cum
        sc_s[rows, :] = scores
        return carry

    lax.fori_loop(0, chunks, forward, 0)
    pl.semaphore_wait(barrier, n_sp - 1)
    mycols = pl.ds(pl.multiple_of(sp * channels, channels), channels)
    copies = []
    for peer, o in peers:
        copies.append(
            pltpu.make_async_remote_copy(
                src_ref=dz_ref.at[pl.ds(pl.multiple_of(peer * tokens, tokens), tokens)],
                dst_ref=oz_ref.at[:, mycols],
                send_sem=z_send.at[o],
                recv_sem=z_recv.at[o],
                device_id={"sp": peer},
                device_id_type=MESH,
            )
        )
        copies[-1].start()
    oz_ref[:, mycols] = dz_ref[pl.ds(pl.multiple_of(sp * tokens, tokens), tokens), :]

    st_s[...] = jnp.zeros_like(st_s)
    du_s[...] = jnp.zeros_like(du_s)
    dbu_s[...] = jnp.zeros_like(dbu_s)
    dcu_s[...] = jnp.zeros_like(dcu_s)
    last = row == BLOCK - 1

    def backward(i, ga):
        c = chunks - 1 - i
        base = pl.multiple_of(c * BLOCK, BLOCK)
        rows = pl.ds(base, BLOCK)
        bb = split(bs_s[rows, :])
        cb = split(cs_s[rows, :])
        ct = split(cs_s[rows, :].T)
        dscores = jnp.zeros((BLOCK, BLOCK), F32)
        dcc = jnp.zeros((BLOCK, STATE), F32)
        dbb = jnp.zeros((BLOCK, STATE), F32)
        racc = jnp.zeros((BLOCK, LANES), F32)
        qacc = jnp.zeros((BLOCK, LANES), F32)
        for j in range(pairs):
            cols = pl.ds(j * LANES, LANES)
            dy = dy_s[rows, cols]
            xdf = xd_s[rows, cols]
            mrows = pl.ds(c * per * BLOCK, per * BLOCK)
            ea = ea_s[rows, cols]
            te = te_s[rows, cols]
            sin = sin_s[pl.ds(c * STATE, STATE), cols]
            ds = st_s[:, cols]
            dsb = split(ds)
            dycat = split(jnp.concatenate([jnp.where(half[k], dy, 0.0) for k in range(per)], axis=0))
            dm = dot3(dycat, split(xdf), ((1,), (1,))) * l_s[j, mrows, :]
            for k in range(per):
                dscores = dscores + dm[k * BLOCK : (k + 1) * BLOCK]
            dstate = te * dot3(bb, dsb)
            dxd = dot3(split(m_s[j, mrows, :].T), dycat) + dstate
            edy = split(ea * dy)
            dcc = dcc + dot3(edy, split(sin), ((1,), (1,)))
            dbb = dbb + dot3(split(xdf * te), dsb, ((1,), (1,)))
            eal = ea[BLOCK - 1 : BLOCK, :]
            st_s[:, cols] = ds * eal + dot3(ct, edy)
            tail = jnp.sum(xdf * dstate, axis=0, keepdims=True) + eal * jnp.sum(
                ds * sin, axis=0, keepdims=True
            )
            r = r_s[rows, cols] - xdf * dxd + jnp.where(last, tail, 0.0)
            xa = xa_s[rows, cols]
            q = dxd * xa
            place = jnp.where(row // head_dim + j * per == lane, 1.0, 0.0).astype(BF16)
            place2 = jnp.concatenate([place, place], axis=0)

            racc = racc + summed(r, place2)
            qacc = qacc + summed(q, place2)
            dxa = dxd * dtp_s[rows, cols] + cp_ref[1:2, cols] * dy
            du = dxa * gx_s[rows, cols]
            dx_ref[rows, cols] = conv_back(du, du_s, tapx_ref[:, cols].astype(F32), cols).astype(BF16)
        dcc = dcc + dot3(split(dscores), bb)
        dbb = dbb + dot3(split(dscores.T), cb)
        every = slice(None)
        tb = tapb_ref[:, pl.ds(gcol, STATE)].astype(F32)
        tc = tapc_ref[:, pl.ds(gcol, STATE)].astype(F32)
        db_ref[rows, :] = conv_back(dbb * gb_s[rows, :], dbu_s, tb, every).astype(BF16)
        dc_ref[rows, :] = conv_back(dcc * gc_s[rows, :], dcu_s, tc, every).astype(BF16)
        dlog = dot(triu, racc, precision=highest)
        ddt = qacc - dlog * decay
        dd_ref[rows, :] = (ddt * dts_s[rows, :]).astype(BF16)
        return ga + jnp.sum(dlog * step_s[rows, :], axis=0, keepdims=True)

    ga = lax.fori_loop(0, chunks, backward, jnp.zeros((1, LANES), F32))
    ga_ref[...] = jnp.broadcast_to(ga, ga_ref.shape)
    for copy in copies:
        copy.wait()


def arrive_kernel(n_sp, cot_ref, out_ref, send, recv):
    tokens = cot_ref.shape[0]
    channels = out_ref.shape[1]
    sp = lax.axis_index("sp")
    peers = [(lax.rem(sp + o, n_sp), o) for o in range(1, n_sp)]
    barrier = pltpu.get_barrier_semaphore()
    for peer, _ in peers:
        pl.semaphore_signal(barrier, inc=1, device_id={"sp": peer}, device_id_type=MESH)
    pl.semaphore_wait(barrier, n_sp - 1)
    ours = pl.ds(pl.multiple_of(sp * tokens, tokens), tokens)
    copies = []
    for peer, o in peers:
        theirs = pl.ds(pl.multiple_of(peer * channels, channels), channels)
        copies.append(
            pltpu.make_async_remote_copy(
                src_ref=cot_ref.at[:, theirs],
                dst_ref=out_ref.at[ours],
                send_sem=send.at[o],
                recv_sem=recv.at[o],
                device_id={"sp": peer},
                device_id_type=MESH,
            )
        )
        copies[-1].start()
    out_ref[ours, :] = cot_ref[:, pl.ds(pl.multiple_of(sp * channels, channels), channels)]
    for copy in copies:
        copy.wait()


def arrive(cot, n_sp):
    tokens, width = cot.shape
    return pl.pallas_call(
        functools.partial(arrive_kernel, n_sp),
        out_shape=jax.ShapeDtypeStruct((tokens * n_sp, width // n_sp), BF16),
        in_specs=[pl.BlockSpec(memory_space=pltpu.VMEM)],
        out_specs=pl.BlockSpec(memory_space=pltpu.VMEM),
        scratch_shapes=[pltpu.SemaphoreType.DMA((n_sp,)), pltpu.SemaphoreType.DMA((n_sp,))],
        compiler_params=pltpu.CompilerParams(collective_id=1, has_side_effects=True),
    )(cot)


def mixer(cot, x, z, b, c, dt, tapx, tapb, tapc, hp, cp, n_sp, group_span, head_dim, heads):
    length, channels = x.shape
    per = LANES // head_dim
    vm = pltpu.VMEM
    wide = vm((length, channels), F32)
    thin = vm((length, LANES), F32)
    return pl.pallas_call(
        functools.partial(mixer_kernel, n_sp, group_span, head_dim, heads),
        out_shape=(
            jax.ShapeDtypeStruct((length, channels), BF16),
            jax.ShapeDtypeStruct((length // n_sp, channels * n_sp), BF16),
            jax.ShapeDtypeStruct((length, STATE), BF16),
            jax.ShapeDtypeStruct((length, STATE), BF16),
            jax.ShapeDtypeStruct((length, LANES), BF16),
            jax.ShapeDtypeStruct((8, LANES), F32),
        ),
        in_specs=[pl.BlockSpec(memory_space=pltpu.VMEM)] * 11,
        out_specs=tuple([pl.BlockSpec(memory_space=pltpu.VMEM)] * 6),
        scratch_shapes=[
            vm((length, channels), BF16),
            pltpu.SemaphoreType.DMA((n_sp,)),
            pltpu.SemaphoreType.DMA((n_sp,)),
            wide,
            wide,
            wide,
            wide,
            wide,
            wide,
            vm((channels // LANES, length * per, LANES), F32),
            vm((channels // LANES, length * per, LANES), F32),
            wide,
            wide,
            vm((8, channels), F32),
            vm((length // BLOCK * STATE, channels), F32),
            vm((STATE, channels), F32),
            thin,
            thin,
            thin,
            thin,
            vm((8, STATE), F32),
            vm((8, STATE), F32),
            thin,
            thin,
            thin,
            thin,
        ],
        compiler_params=pltpu.CompilerParams(
            collective_id=2, has_side_effects=True, vmem_limit_bytes=50 * 1024 * 1024
        ),
    )(cot, x, z, b, c, dt, tapx, tapb, tapc, hp, cp)


def exchange_kernel(
    n_sp,
    n_dp,
    group_span,
    heads,
    reduce_here,
    dx_ref,
    db_ref,
    dc_ref,
    dd_ref,
    ga_ref,
    li_ref,
    ox_ref,
    ob_ref,
    oc_ref,
    od_ref,
    oga_ref,
    ow_ref,
    rb,
    rc,
    rd,
    rga,
    part,
    rs1,
    mine1,
    rs2,
    mine2,
    rs3,
    ex_send,
    ex_recv,
    ga_send,
    ga_recv,
    w_send,
    w_recv,
    v_send,
    v_recv,
):
    tokens = ox_ref.shape[0]
    channels = dx_ref.shape[1]
    sp = lax.axis_index("sp")
    dp = lax.axis_index("dp")
    sp_peers = [(lax.rem(sp + o, n_sp), o) for o in range(1, n_sp)]
    dp_peers = [(lax.rem(dp + o, n_dp), o) for o in range(1, n_dp)]

    barrier = pltpu.get_barrier_semaphore()
    for peer, _ in sp_peers:
        pl.semaphore_signal(barrier, inc=1, device_id={"sp": peer}, device_id_type=MESH)
    waits = n_sp - 1
    if reduce_here:
        for peer, _ in dp_peers:
            pl.semaphore_signal(barrier, inc=1, device_id={"dp": peer}, device_id_type=MESH)
        waits += n_dp - 1
    pl.semaphore_wait(barrier, waits)

    def to_sp(src, dst, slot, o, peer, send, recv):
        return pltpu.make_async_remote_copy(
            src_ref=src,
            dst_ref=dst,
            send_sem=send.at[slot, o],
            recv_sem=recv.at[slot, o],
            device_id={"sp": peer},
            device_id_type=MESH,
        )

    def to_dp(src, dst, slot, o, peer, send, recv):
        return pltpu.make_async_remote_copy(
            src_ref=src,
            dst_ref=dst,
            send_sem=send.at[slot, o],
            recv_sem=recv.at[slot, o],
            device_id={"dp": peer},
            device_id_type=MESH,
        )

    mycols = pl.ds(pl.multiple_of(sp * channels, channels), channels)
    first, second, sums = [], [], []
    for peer, o in sp_peers:
        theirs = pl.ds(pl.multiple_of(peer * tokens, tokens), tokens)
        first.append(to_sp(dd_ref.at[theirs], rd.at[sp], 0, o, peer, ex_send, ex_recv))
        second.append(to_sp(db_ref.at[theirs], rb.at[sp], 1, o, peer, ex_send, ex_recv))
        second.append(to_sp(dc_ref.at[theirs], rc.at[sp], 2, o, peer, ex_send, ex_recv))
        second.append(to_sp(dx_ref.at[theirs], ox_ref.at[:, mycols], 3, o, peer, ex_send, ex_recv))
    for copy in first:
        copy.start()
    if reduce_here:
        for peer, o in dp_peers:
            sums.append(to_dp(ga_ref, rga.at[dp], 0, o, peer, ga_send, ga_recv))
            sums[-1].start()
    for copy in second:
        copy.start()
    ours = pl.ds(pl.multiple_of(sp * tokens, tokens), tokens)
    ox_ref[:, mycols] = dx_ref[ours, :]
    rb[sp] = db_ref[ours, :]
    rc[sp] = dc_ref[ours, :]
    rd[sp] = dd_ref[ours, :]
    for copy in first:
        copy.wait()
    heads_here = heads // n_sp
    dd = rd[0].astype(F32)
    for k in range(1, n_sp):
        dd = dd + pltpu.roll(rd[k].astype(F32), k * heads_here, 1)
    od_ref[...] = dd
    whole = dot(dd.astype(BF16), li_ref[...], ((0,), (0,)))[:heads]
    if reduce_here:
        part[...] = whole.astype(BF16)
        width = part.shape[1] // n_dp
        mcols = pl.ds(pl.multiple_of(dp * width, width), width)
        steps = []
        for peer, o in dp_peers:
            theirs = pl.ds(pl.multiple_of(peer * width, width), width)
            steps.append(to_dp(part.at[:, theirs], rs1.at[dp], 0, o, peer, v_send, v_recv))
            steps[-1].start()
        rs1[dp] = part[:, mcols]
        for copy in steps:
            copy.wait()
        mine1[...] = functools.reduce(lambda a, b: a + b, [rs1[k].astype(F32) for k in range(n_dp)])
        steps = []
        for peer, o in sp_peers:
            steps.append(to_sp(mine1, rs2.at[sp], 0, o, peer, w_send, w_recv))
            steps[-1].start()
        rs2[sp] = mine1[...]
        for copy in steps:
            copy.wait()
        total = functools.reduce(lambda a, b: a + b, [rs2[k] for k in range(n_sp)])
        mine2[...] = total.astype(BF16)
        steps = []
        for peer, o in dp_peers:
            steps.append(to_dp(mine2, rs3.at[dp], 1, o, peer, v_send, v_recv))
            steps[-1].start()
        rs3[dp] = mine2[...]
        rga[dp] = ga_ref[...]
        for copy in sums:
            copy.wait()
        oga_ref[...] = functools.reduce(lambda a, b: a + b, [rga[k] for k in range(n_dp)])
        for copy in steps:
            copy.wait()
        for k in range(n_dp):
            ow_ref[:, k * width : (k + 1) * width] = rs3[k].astype(F32)
    else:
        ow_ref[...] = whole
        oga_ref[...] = ga_ref[...]
    for copy in second:
        copy.wait()
    for out, slots in ((ob_ref, rb), (oc_ref, rc)):
        for g in range(GROUPS):
            total = slots[g * group_span].astype(F32)
            for k in range(1, group_span):
                total = total + slots[g * group_span + k].astype(F32)
            out[:, g * STATE : (g + 1) * STATE] = total.astype(BF16)


def exchange(dx, db, dc, dd, ga, li, n_sp, n_dp, group_span, heads, reduce_here):
    tokens, width = li.shape
    channels = dx.shape[1]
    vm = pltpu.VMEM
    dma = pltpu.SemaphoreType.DMA
    return pl.pallas_call(
        functools.partial(exchange_kernel, n_sp, n_dp, group_span, heads, reduce_here),
        out_shape=(
            jax.ShapeDtypeStruct((tokens, channels * n_sp), BF16),
            jax.ShapeDtypeStruct((tokens, GROUPS * STATE), BF16),
            jax.ShapeDtypeStruct((tokens, GROUPS * STATE), BF16),
            jax.ShapeDtypeStruct((tokens, LANES), F32),
            jax.ShapeDtypeStruct((8, LANES), F32),
            jax.ShapeDtypeStruct((heads, width), F32),
        ),
        in_specs=[pl.BlockSpec(memory_space=pltpu.VMEM)] * 6,
        out_specs=tuple([pl.BlockSpec(memory_space=pltpu.VMEM)] * 6),
        scratch_shapes=[
            vm((n_sp, tokens, STATE), BF16),
            vm((n_sp, tokens, STATE), BF16),
            vm((n_sp, tokens, LANES), BF16),
            vm((n_dp, 8, LANES), F32),
            vm((heads, width), BF16),
            vm((n_dp, heads, width // n_dp), BF16),
            vm((heads, width // n_dp), F32),
            vm((n_sp, heads, width // n_dp), F32),
            vm((heads, width // n_dp), BF16),
            vm((n_dp, heads, width // n_dp), BF16),
            dma((4, n_sp)),
            dma((4, n_sp)),
            dma((1, n_dp)),
            dma((1, n_dp)),
            dma((2, n_sp)),
            dma((2, n_sp)),
            dma((2, n_dp)),
            dma((2, n_dp)),
        ],
        compiler_params=pltpu.CompilerParams(
            collective_id=0, has_side_effects=True, vmem_limit_bytes=40 * 1024 * 1024
        ),
    )(dx, db, dc, dd, ga, li)


def shards(
    cotangent,
    layer_input,
    x_pre,
    z_pre,
    b_pre,
    c_pre,
    dt_raw,
    conv_x,
    conv_b,
    conv_c,
    dt_bias,
    a_log,
    d_skip,
    norm_w,
):
    n_sp = lax.axis_size("sp")
    n_dp = lax.axis_size("dp")
    seqs = x_pre.shape[0]
    assert seqs == 1
    heads_here = dt_raw.shape[2]
    heads = heads_here * n_sp
    head_dim = x_pre.shape[2] // heads_here
    group_span = n_sp // GROUPS
    arrived = arrive(cotangent[0], n_sp)
    dt = jnp.pad(dt_raw[0], ((0, 0), (0, LANES - heads_here)))
    hp = jnp.pad(jnp.stack([dt_bias, a_log]), ((0, 0), (0, LANES - heads_here)))
    cp = jnp.stack([norm_w, jnp.repeat(d_skip, head_dim)])
    dx, oz, db, dc, dd, ga = mixer(
        arrived, x_pre[0], z_pre[0], b_pre[0], c_pre[0], dt, conv_x, conv_b, conv_c, hp, cp,
        n_sp, group_span, head_dim, heads_here,
    )
    reduce_here = heads % 16 == 0 and (layer_input.shape[2] // n_dp) % LANES == 0
    ox, ob, oc, od, oga, ow = exchange(
        dx, db, dc, dd, ga, layer_input[0], n_sp, n_dp, group_span, heads, reduce_here
    )
    grad_a_log = oga[0, :heads_here]
    if not reduce_here:
        ow, grad_a_log = lax.psum((ow, grad_a_log), "dp")
        ow = lax.psum(ow, "sp")
    return (
        ox[None],
        oz[None],
        ob[None],
        oc[None],
        od[None, :, :heads].astype(BF16),
        grad_a_log,
        ow.T,
    )


def solution(mesh):
    placed = (
        P("dp", "sp", None),
        P("dp", "sp", None),
        P("dp", None, "sp"),
        P("dp", None, "sp"),
        P("dp", None, None),
        P("dp", None, None),
        P("dp", None, "sp"),
        P(None, "sp"),
        P(),
        P(),
        P("sp"),
        P("sp"),
        P("sp"),
        P("sp"),
    )
    return jax.shard_map(
        shards,
        mesh=mesh,
        in_specs=placed,
        out_specs=(
            P("dp", "sp", None),
            P("dp", "sp", None),
            P("dp", "sp", None),
            P("dp", "sp", None),
            P("dp", "sp", None),
            P("sp"),
            P(),
        ),
        check_vma=False,
    )
```

profile of v0, /device:TPU:0, one launch (start us, length us, event | category | flops | bytes accessed | tf_op | source)
XLA Modules:
  0.0 58.6 jit_solution(16331834356584941727)
XLA Ops:
  0.6 0.0 copy-start.12
  0.6 0.0 copy-start.13
  0.7 0.6 %copy-done.12 = f32[8]{0:T(128)S(1)} copy-done((f32[8]{0:T(128)S(1)}, f32[8]{0:T(128)}, u32[]{:S(2)}) %copy-start.12) | copy-done | bytes 56
  1.3 0.0 copy-done.13
  1.3 0.6 %copy-done.11 = f32[8]{0:T(128)S(1)} copy-done((f32[8]{0:T(128)S(1)}, f32[8]{0:T(128)}, u32[]{:S(2)}) %copy-start.11) | copy-done | bytes 56
  2.0 0.1 broadcast_in_dim.16
  2.0 0.1 stack_reshape.3
  2.1 0.5 copy-done.10
  2.7 0.1 copy-done.9
  2.7 0.2 copy.21
  2.9 0.0 copy-start.4
  2.9 0.0 copy-start.1
  3.0 0.0 copy-start.2
  3.0 11.1 %shard_map.189.cot_ref = bf16[512,512]{1,0:T(8,128)(2,1)} custom-call(bf16[128,2048]{1,0:T(8,128)(2,1)} %bitcast.29), custom_call_target="tpu_custom_call" | custom-call | tf_op jit(solution)/shard_map/pallas_call | solution.py:342
  14.1 0.0 copy-done.6
  14.1 0.0 copy-done.7
  14.1 0.0 copy-done.8
  14.1 0.0 copy-done.4
  14.1 0.0 copy-done.1
  14.1 0.0 copy-done.2
  14.2 1.0 %copy-done = bf16[512,512]{1,0:T(8,128)(2,1)S(1)} copy-done((bf16[512,512]{1,0:T(8,128)(2,1)S(1)}, bf16[512,512]{1,0:T(8,128)(2,1)}, u32[]{:S(2)}) %copy-start) | copy-done | bytes 524312
  15.2 0.9 %copy-done.5 = bf16[1,512,256]{2,1,0:T(8,128)(2,1)S(1)} copy-done((bf16[1,512,256]{2,1,0:T(8,128)(2,1)S(1)}, bf16[1,512,256]{2,1,0:T(8,128)(2,1)}, u32[]{:S(2)}) %copy-start.5) | copy-done | bytes 262168
  16.1 15.2 %shard_map.190 = (bf16[512,512]{1,0:T(8,128)(2,1)S(1)}, bf16[128,2048]{1,0:T(8,128)(2,1)S(1)}, bf16[512,128]{1,0:T(8,128)(2,1)S(1)}, bf16[512,128]{1,0:T(8,128)(...) custom-call(bf16[512,512]{1,0:T(8,128)(2,1)S(1)} %copy-done, bf16[512,512]{1,0:T(8,128)(2,1)S(1)} %bitcast.21, ...), custom_call_target="tpu_custom_call" | custom-call | tf_op jit(solution)/shard_map/pallas_call | solution.py:358
  31.3 0.0 copy-done.3
  31.4 22.5 %shard_map.191 = (bf16[128,2048]{1,0:T(8,128)(2,1)S(1)}, bf16[128,256]{1,0:T(8,128)(2,1)S(1)}, bf16[128,256]{1,0:T(8,128)(2,1)S(1)}, f32[128,128]{1,0:T(8,128)S(...) custom-call(bf16[512,512]{1,0:T(8,128)(2,1)S(1)} %get-tuple-element.19.dx_ref, ...), custom_call_target="tpu_custom_call" | custom-call | tf_op jit(solution)/shard_map/pallas_call | solution.py:560
  53.8 0.5 slice_bitcast_fusion
  54.3 0.7 %copy.22 = bf16[1,128,32]{1,2,0:T(8,128)(2,1)} copy(bf16[1,128,32]{2,1,0:T(8,128)(2,1)S(1)} %fusion) | data formatting | bytes 16384
  55.0 0.8 %copy.28 = bf16[1,128,2048]{2,1,0:T(8,128)(2,1)} copy(bf16[1,128,2048]{2,1,0:T(8,128)(2,1)S(1)} %bitcast.20) | data formatting | bytes 1048576
  55.8 0.8 %copy.29 = bf16[1,128,2048]{2,1,0:T(8,128)(2,1)} copy(bf16[1,128,2048]{2,1,0:T(8,128)(2,1)S(1)} %bitcast.19) | data formatting | bytes 1048576
  56.6 0.6 %copy.30 = bf16[1,128,256]{2,1,0:T(8,128)(2,1)} copy(bf16[1,128,256]{2,1,0:T(8,128)(2,1)S(1)} %bitcast.28) | data formatting | bytes 131072
  57.2 0.6 %copy.31 = bf16[1,128,256]{2,1,0:T(8,128)(2,1)} copy(bf16[1,128,256]{2,1,0:T(8,128)(2,1)S(1)} %bitcast.27) | data formatting | bytes 131072
  57.9 0.7 %copy.32 = f32[2048,32]{0,1:T(8,128)} copy(f32[2048,32]{0,1:T(8,128)S(1)} %bitcast.24) | data formatting | bytes 524288
  (13 shorter events, 0.1 us)
Async XLA Ops:
  0.6 0.7 %copy-start.12 = (f32[8]{0:T(128)S(1)}, f32[8]{0:T(128)}, u32[]{:S(2)}) copy-start(f32[8]{0:T(128)} %param.25) | copy-start | bytes 100
  0.6 0.7 %copy-start.13 = (f32[8]{0:T(128)S(1)}, f32[8]{0:T(128)}, u32[]{:S(2)}) copy-start(f32[8]{0:T(128)} %param.24) | copy-start | bytes 100
  1.3 0.7 %copy-start.11 = (f32[8]{0:T(128)S(1)}, f32[8]{0:T(128)}, u32[]{:S(2)}) copy-start(f32[8]{0:T(128)} %param.26) | copy-start | bytes 100
  2.0 0.7 %copy-start.10 = (f32[512]{0:T(512)S(1)}, f32[512]{0:T(512)}, u32[]{:S(2)}) copy-start(f32[512]{0:T(512)} %param.27) | copy-start | bytes 6148
  2.0 0.7 %copy-start.9 = (bf16[1,512,8]{1,2,0:T(8,128)(2,1)S(1)}, bf16[1,512,8]{1,2,0:T(8,128)(2,1)}, u32[]{:S(2)}) copy-start(bf16[1,512,8]{1,2,0:T(8,128)(2,1)} %param.20) | copy-start | bytes 24580
  2.7 11.4 %copy-start.6 = (bf16[4,512]{1,0:T(4,128)(2,1)S(1)}, bf16[4,512]{1,0:T(4,128)(2,1)}, u32[]{:S(2)}) copy-start(bf16[4,512]{1,0:T(4,128)(2,1)} %tapx_ref.1) | copy-start | bytes 12292
  2.7 11.4 %copy-start.7 = (bf16[4,256]{1,0:T(4,128)(2,1)S(1)}, bf16[4,256]{1,0:T(4,128)(2,1)}, u32[]{:S(2)}) copy-start(bf16[4,256]{1,0:T(4,128)(2,1)} %tapb_ref.1) | copy-start | bytes 6148
  2.7 11.4 %copy-start.8 = (bf16[4,256]{1,0:T(4,128)(2,1)S(1)}, bf16[4,256]{1,0:T(4,128)(2,1)}, u32[]{:S(2)}) copy-start(bf16[4,256]{1,0:T(4,128)(2,1)} %tapc_ref.1) | copy-start | bytes 6148
  2.9 11.2 %copy-start.4 = (bf16[1,512,256]{2,1,0:T(8,128)(2,1)S(1)}, bf16[1,512,256]{2,1,0:T(8,128)(2,1)}, u32[]{:S(2)}) copy-start(bf16[1,512,256]{2,1,0:T(8,128)(2,1)} %param.18) | copy-start | bytes 786436
  2.9 11.2 %copy-start.1 = (bf16[1,512,512]{2,1,0:T(8,128)(2,1)S(1)}, bf16[1,512,512]{2,1,0:T(8,128)(2,1)}, u32[]{:S(2)}) copy-start(bf16[1,512,512]{2,1,0:T(8,128)(2,1)} %param.16) | copy-start | bytes 1572868
  3.0 11.2 %copy-start.2 = (bf16[1,512,512]{2,1,0:T(8,128)(2,1)S(1)}, bf16[1,512,512]{2,1,0:T(8,128)(2,1)}, u32[]{:S(2)}) copy-start(bf16[1,512,512]{2,1,0:T(8,128)(2,1)} %param.17) | copy-start | bytes 1572868
  14.1 1.0 %copy-start = (bf16[512,512]{1,0:T(8,128)(2,1)S(1)}, bf16[512,512]{1,0:T(8,128)(2,1)}, u32[]{:S(2)}) copy-start(bf16[512,512]{1,0:T(8,128)(2,1)} %shard_map.189.cot_ref) | copy-start | bytes 1572868
  15.2 0.9 %copy-start.5 = (bf16[1,512,256]{2,1,0:T(8,128)(2,1)S(1)}, bf16[1,512,256]{2,1,0:T(8,128)(2,1)}, u32[]{:S(2)}) copy-start(bf16[1,512,256]{2,1,0:T(8,128)(2,1)} %param.19) | copy-start | bytes 786436
  16.1 15.2 %copy-start.3 = (bf16[1,128,2048]{2,1,0:T(8,128)(2,1)S(1)}, bf16[1,128,2048]{2,1,0:T(8,128)(2,1)}, u32[]{:S(2)}) copy-start(bf16[1,128,2048]{2,1,0:T(8,128)(2,1)} %param.15) | copy-start | bytes 1572868
where the time goes:
time: 58.9 us; the launch traced here: 58.6 us
  Pallas kernels  48.8 us (83%)
  local copies, waits for them, and re-layouts  9.01 us (15%)
  between operations  0.79 us (1%)
    pallas_call x1, Pallas kernels, exchange(): pl.pallas_call(functools.partial(exchange_kernel, n_sp, n_dp, group_span,...  22.5 us
    pallas_call x1, Pallas kernels, mixer(): pl.pallas_call(functools.partial(mixer_kernel, n_sp, group_span, head_dim...  15.2 us
    pallas_call x1, Pallas kernels, arrive(): pl.pallas_call(functools.partial(arrive_kernel, n_sp), out_shape=jax.Shap...  11.1 us
    unnamed x35, local copies, waits for them, and re-layouts  8.31 us

commit v1 on v0

v1 whole, which is shorter than its diff:
```python
import functools

import jax
import jax.numpy as jnp
from jax import lax
from jax.experimental import pallas as pl
from jax.experimental.pallas import tpu as pltpu
from jax.sharding import PartitionSpec as P

GROUPS = 2
STATE = 128
BLOCK = 128
LANES = 128
ROWS = 8
PAD = 8
CUT = 1
WAVE = 4
EPS = 1e-05
LOG2E = 1.4426950408889634
MESH = pl.DeviceIdType.MESH
F32 = jnp.float32
BF16 = jnp.bfloat16
ROWS_ROWS = ((1,), (1,))
COLS_COLS = ((0,), (0,))


def dot(a, b, dims=((1,), (0,)), precision=None):
    return lax.dot_general(a, b, (dims, ((), ())), precision=precision, preferred_element_type=F32)


def iota(axis, shape=(BLOCK, LANES)):
    return lax.broadcasted_iota(jnp.int32, shape, axis)


def silu_parts(u):
    sig = jax.nn.sigmoid(u)
    act = u * sig
    return act, sig + act * (1.0 - sig)


def halves(v):
    hi = v.astype(BF16)
    return jnp.concatenate([hi, (v - hi.astype(F32)).astype(BF16)], axis=1)


def add_all(parts):
    return functools.reduce(lambda a, b: a + b, parts)


def step_kernel(
    n_sp,
    n_dp,
    group_span,
    head_dim,
    heads,
    reduce_here,
    cot_hbm,
    li_hbm,
    x_hbm,
    z_hbm,
    b_hbm,
    c_hbm,
    dt_hbm,
    tapx_hbm,
    tapb_hbm,
    tapc_hbm,
    bias_hbm,
    alog_hbm,
    skip_hbm,
    nw_hbm,
    ox_ref,
    oz_ref,
    ob_ref,
    oc_ref,
    od_ref,
    oga_ref,
    ow_ref,
    cot_v,
    li_v,
    x_v,
    z_v,
    b_v,
    c_v,
    dt_v,
    tapx_v,
    tapb_v,
    tapc_v,
    bias_v,
    alog_v,
    skip_v,
    nw_v,
    cotr_s,
    xf_s,
    bf_s,
    cf_s,
    xa_s,
    gx_s,
    y_s,
    dtp_s,
    ea_s,
    te_s,
    sin_s,
    ds_s,
    st_s,
    lam_s,
    m_s,
    xdb_s,
    xdte_s,
    dy_s,
    edy_s,
    du_s,
    bb_s,
    cb_s,
    gb_s,
    gc_s,
    ct_s,
    dbu_s,
    dcu_s,
    cp_s,
    dtt_s,
    step_s,
    cum_s,
    sig_s,
    ga_s,
    acc_s,
    dyf_s,
    dsf_s,
    dz_s,
    dx_s,
    dbc_s,
    dd_s,
    rbc,
    rd,
    rga,
    part,
    rs1,
    mine1,
    rs2,
    mine2,
    rs3,
    in_sem,
    cot_send,
    cot_recv,
    z_send,
    z_recv,
    x_send,
    x_recv,
    bc_send,
    bc_recv,
    d_send,
    d_recv,
    ga_send,
    ga_recv,
    w1_send,
    w1_recv,
    w2_send,
    w2_recv,
    w3_send,
    w3_recv,
):
    pairs, length, _ = x_v.shape
    channels = pairs * LANES
    tokens = oz_ref.shape[0]
    chunks = length // BLOCK
    per = LANES // head_dim
    sp = lax.axis_index("sp")
    dp = lax.axis_index("dp")
    sp_peers = [lax.rem(sp + o, n_sp) for o in range(1, n_sp)]
    dp_peers = [lax.rem(dp + o, n_dp) for o in range(1, n_dp)] if reduce_here else []
    gcol = pl.multiple_of((sp // group_span) * STATE, STATE)
    gcols = pl.ds(gcol, STATE)

    def block(c, size=BLOCK):
        return pl.ds(pl.multiple_of(c * size, size), size)

    ours = block(sp, tokens)

    loads = {}

    def load(name, src, dst):
        loads[name] = loads.get(name, []) + [pltpu.make_async_copy(src, dst, in_sem.at[sum(map(len, loads.values()))])]
        loads[name][-1].start()

    def arrived(*names):
        for name in names:
            for copy in loads[name]:
                copy.wait()

    load("dt", dt_hbm, dt_v)
    load("dt", bias_hbm, bias_v)
    load("dt", alog_hbm, alog_v)
    load("bc", b_hbm.at[:, gcols], b_v)
    load("bc", c_hbm.at[:, gcols], c_v)
    load("bc", tapb_hbm, tapb_v)
    load("bc", tapc_hbm, tapc_v)
    load("x", tapx_hbm, tapx_v)
    load("x", skip_hbm, skip_v)
    load("x", nw_hbm, nw_v)
    for j in range(pairs):
        load("x", x_hbm.at[:, pl.ds(j * LANES, LANES)], x_v.at[j])
    load("cot", cot_hbm, cot_v)
    for j in range(pairs):
        load("z", z_hbm.at[:, pl.ds(j * LANES, LANES)], z_v.at[j])
    load("li", li_hbm, li_v)

    barrier = pltpu.get_barrier_semaphore()
    for peer in sp_peers:
        pl.semaphore_signal(barrier, inc=1, device_id={"sp": peer}, device_id_type=MESH)
    for peer in dp_peers:
        pl.semaphore_signal(barrier, inc=1, device_id={"dp": peer}, device_id_type=MESH)

    def remote(src, dst, send, recv, axis, peer):
        return pltpu.make_async_remote_copy(
            src_ref=src, dst_ref=dst, send_sem=send, recv_sem=recv,
            device_id={axis: peer}, device_id_type=MESH,
        )

    def cot_copy(peer, recv, j):
        return remote(
            cot_v.at[:, block(peer * pairs + j, LANES)], cotr_s.at[j, block(recv, tokens)],
            cot_send.at[peer, j], cot_recv.at[recv, j], "sp", peer,
        )

    def z_copy(peer, recv, j):
        return remote(
            dz_s.at[j, block(peer, tokens)], oz_ref.at[:, block(recv * pairs + j, LANES)],
            z_send.at[peer, j], z_recv.at[recv, j], "sp", peer,
        )

    def x_copy(peer, recv, j):
        return remote(
            dx_s.at[j, block(peer, tokens)], ox_ref.at[:, block(recv * pairs + j, LANES)],
            x_send.at[peer, j], x_recv.at[recv, j], "sp", peer,
        )

    def bc_copy(peer, recv):
        return remote(
            dbc_s.at[block(peer, tokens)], rbc.at[recv], bc_send.at[peer], bc_recv.at[recv], "sp", peer,
        )

    def d_copy(peer, recv):
        return remote(dd_s.at[peer], rd.at[recv], d_send.at[peer], d_recv.at[recv], "sp", peer)

    lane = iota(1)
    row = iota(0)
    half = [lane // head_dim == k for k in range(per)]
    half_b = [jnp.where(iota(1, (1, LANES)) // head_dim == k, 1.0, 0.0).astype(BF16) for k in range(per)]
    causal = row >= lane
    tri = jnp.where(causal, 1.0, 0.0).astype(BF16)
    same = jnp.where(row // head_dim == lane // head_dim, 1.0 / head_dim, 0.0).astype(BF16)
    same = jnp.concatenate([same, same], axis=0)

    def pick(parts):
        out = parts[-1]
        for k in range(per - 1):
            out = jnp.where(half[k][: out.shape[0]], parts[k], out)
        return out

    def column(v):
        v = v[...]
        n = v.shape[1]
        diag = iota(0, (ROWS, n)) == iota(1, (ROWS, n))
        return jnp.sum(jnp.where(diag, jnp.broadcast_to(v, (ROWS, n)), 0.0), axis=1, keepdims=True)

    arrived("dt")
    decay = jnp.exp(column(alog_v))
    raw = dt_v[...].astype(F32)
    if heads < ROWS:
        raw = jnp.concatenate([raw, jnp.zeros((ROWS - heads, length), F32)], axis=0)
    pre = raw + column(bias_v)
    live = iota(0, (ROWS, length)) < heads
    dt = jnp.where(live, jnp.maximum(pre, 0.0) + jnp.log1p(jnp.exp(-jnp.abs(pre))), 0.0)
    dtt_s[...] = dt
    step_s[...] = -dt * decay
    sig_s[...] = jax.nn.sigmoid(pre)
    log_step = dt * (-LOG2E * decay)
    log_step = jnp.concatenate([log_step[:, c * BLOCK : (c + 1) * BLOCK] for c in range(chunks)], axis=0)
    first = log_step.astype(BF16)
    rest = log_step - first.astype(F32)
    triu = jnp.where(row <= lane, 1.0, 0.0).astype(BF16)
    cum_s[...] = dot(
        jnp.concatenate([first, halves(rest)], axis=1), jnp.concatenate([triu, triu, triu], axis=0)
    )
    arrived("bc", "x")

    cp_s[0:1, :] = nw_v[...]
    skip = skip_v[...]
    for j in range(pairs):
        cp_s[1:2, j * LANES : (j + 1) * LANES] = pick(
            [jnp.broadcast_to(skip[0:1, j * per + k : j * per + k + 1], (1, LANES)) for k in range(per)]
        )

    zeros8 = jnp.zeros((PAD, LANES), F32)
    bf_s[0:PAD, :] = zeros8
    cf_s[0:PAD, :] = zeros8
    dbu_s[length : length + PAD, :] = zeros8
    dcu_s[length : length + PAD, :] = zeros8
    for j in range(pairs):
        xf_s[j, 0:PAD, :] = zeros8
        du_s[j, length : length + PAD, :] = zeros8
    st_s[...] = jnp.zeros_like(st_s)

    def conv(ref, base, taps):
        n = taps.shape[0]
        return add_all(
            [ref[pl.ds(base + (PAD - (n - 1 - k)), BLOCK), :] * taps[k : k + 1] for k in range(n)]
        )

    def conv_back(ref, base, taps):
        n = taps.shape[0]
        return add_all([ref[pl.ds(base + (n - 1 - k), BLOCK), :] * taps[k : k + 1] for k in range(n)])

    def forward(c, carry):
        @pl.when(c == min(CUT, chunks - 1))
        def _():
            pl.semaphore_wait(barrier, len(sp_peers) + len(dp_peers))
            arrived("cot")
            for j in range(pairs):
                for peer in sp_peers:
                    cot_copy(peer, sp, j).start()

        base = pl.multiple_of(c * BLOCK, BLOCK)
        rows = pl.ds(base, BLOCK)
        padded = pl.ds(base + PAD, BLOCK)
        bf_s[padded, :] = b_v[rows, :].astype(F32)
        cf_s[padded, :] = c_v[rows, :].astype(F32)
        for j in range(pairs):
            xf_s[j, padded, :] = x_v[j, rows, :].astype(F32)
        ba, gb = silu_parts(conv(bf_s, base, tapb_v[:, gcols].astype(F32)))
        ca, gc = silu_parts(conv(cf_s, base, tapc_v[:, gcols].astype(F32)))
        gb_s[rows, :] = gb
        gc_s[rows, :] = gc
        bb = ba.astype(BF16)
        cb = ca.astype(BF16)
        bb_s[rows, :] = bb
        cb_s[rows, :] = cb
        ct_s[rows, :] = ca.T.astype(BF16)
        b2 = halves(ba)
        c2 = halves(ca)
        c3 = jnp.concatenate([c2, cb], axis=1)
        scores = dot(c3, jnp.concatenate([bb, bb, b2[:, STATE:]], axis=1), ROWS_ROWS)
        bt2 = halves(ba.T)
        dt_c = dtt_s[:, rows]
        cum = cum_s[pl.ds(pl.multiple_of(c * ROWS, ROWS), ROWS), :]
        cols_t = jnp.concatenate([cum, dt_c, jnp.zeros((LANES - 2 * ROWS, LANES), F32)], axis=0).T
        for j in range(pairs):
            cols = pl.ds(j * LANES, LANES)
            xa, gx = silu_parts(conv(xf_s.at[j], base, tapx_v[:, cols].astype(F32)))
            gx_s[j, rows, :] = gx
            xa_s[j, rows, :] = xa
            acols, dcols, his, los = [], [], [], []
            for k in range(per):
                h = j * per + k
                acol = jnp.broadcast_to(cols_t[:, h : h + 1], (BLOCK, LANES))
                acols.append(acol)
                dcols.append(jnp.broadcast_to(cols_t[:, ROWS + h : ROWS + h + 1], (BLOCK, LANES)))
                lam = jnp.exp2(jnp.where(causal, acol - cum[h : h + 1, :], -jnp.inf))
                m = scores * lam
                hi = m.astype(BF16)
                his.append(hi)
                los.append((m - hi.astype(F32)).astype(BF16))
                lam_s[j, rows, k * BLOCK : (k + 1) * BLOCK] = lam
                m_s[j, rows, k * BLOCK : (k + 1) * BLOCK] = hi
            ap = pick(acols)
            dtp = pick(dcols)
            dtp_s[j, rows, :] = dtp
            ea = jnp.exp2(ap)
            te = jnp.exp2(ap[BLOCK - 1 : BLOCK, :] - ap)
            ea_s[j, rows, :] = ea
            te_s[j, rows, :] = te
            xd = xa * dtp
            xd_hi = xd.astype(BF16)
            xd_lo = (xd - xd_hi.astype(F32)).astype(BF16)
            xdte = (xd * te).astype(BF16)
            xdb_s[j, rows, :] = xd_hi
            xdte_s[j, rows, :] = xdte
            cat_hi = [xd_hi * h for h in half_b]
            y = dot(
                jnp.concatenate(his + los + his, axis=1),
                jnp.concatenate(cat_hi + cat_hi + [xd_lo * h for h in half_b], axis=0),
            )
            st = st_s[j]
            sin_s[j, rows, :] = st
            st_hi = st.astype(BF16)
            st_lo = (st - st_hi.astype(F32)).astype(BF16)
            y_s[j, rows, :] = y + dot(c3, jnp.concatenate([st_hi, st_hi, st_lo], axis=0)) * ea
            st_s[j] = st * ea[BLOCK - 1 : BLOCK, :] + dot(bt2, jnp.concatenate([xdte, xdte], axis=0))
        return carry

    lax.fori_loop(0, chunks, forward, 0)

    for j in range(pairs):
        cotr_s[j, ours, :] = cot_v[:, block(sp * pairs + j, LANES)]
    arrived("z")
    acc_s[...] = jnp.zeros_like(acc_s)

    def middle(j, carry):
        cols = block(j, LANES)
        for peer in sp_peers:
            cot_copy(peer, peer, j).wait_recv()
        gain = cp_s[0:1, cols]
        skips = cp_s[1:2, cols]
        place_r = jnp.where(row // head_dim + j * per == lane, 1.0, 0.0).astype(BF16)
        place_q = jnp.where(row // head_dim + (j * per + LANES // 2) == lane, 1.0, 0.0).astype(BF16)
        place_r = jnp.concatenate([place_r, place_r], axis=0)
        for start in range(0, chunks, WAVE):
            wave = list(reversed(range(chunks)))[start : start + WAVE]
            state = []
            for c in wave:
                rows = pl.ds(c * BLOCK, BLOCK)
                full = y_s[j, rows, :] + skips * xa_s[j, rows, :]
                sz, gz = silu_parts(z_v[j, rows, :].astype(F32))
                gated = full * sz
                state.append((full, sz, gz, gated, dot(halves(gated * gated), same)))
            means = []
            for c, (full, sz, gz, gated, power) in zip(wave, state):
                inv = lax.rsqrt(power + EPS)
                gh = gated * inv
                g = cotr_s[j, pl.ds(c * BLOCK, BLOCK), :].astype(F32) * gain
                means.append((inv, gh, g, dot(halves(g * gh), same)))
            for c, (full, sz, gz, gated, _), (inv, gh, g, mean) in zip(wave, state, means):
                rows = pl.ds(c * BLOCK, BLOCK)
                dgated = inv * (g - gh * mean)
                dz_s[j, rows, :] = (dgated * full * gz).astype(BF16)
                dy = dgated * sz
                dyf_s[rows, :] = dy
                dy_s[j, rows, :] = halves(dy)
                edy_s[j, rows, :] = (ea_s[j, rows, :] * dy).astype(BF16)
        ds = jnp.zeros((STATE, LANES), F32)
        for c in reversed(range(chunks)):
            rows = pl.ds(c * BLOCK, BLOCK)
            dsf_s[rows, :] = ds
            ds_s[j, rows, :] = ds.astype(BF16)
            if c > 0:
                last = pl.ds(c * BLOCK + BLOCK - 1, 1)
                ds = ds * ea_s[j, last, :] + dot(ct_s[rows, :], edy_s[j, rows, :])
        for c in reversed(range(chunks)):
            rows = pl.ds(c * BLOCK, BLOCK)
            dy2 = dy_s[j, rows, :]
            mt = jnp.concatenate(
                [m_s[j, rows, k * BLOCK : (k + 1) * BLOCK].astype(F32).T.astype(BF16) for k in range(per)], axis=1
            )
            dycat = [dy2[:, p * LANES : (p + 1) * LANES] * h for p in range(2) for h in half_b]
            dstate = te_s[j, rows, :] * dot(bb_s[rows, :], ds_s[j, rows, :])
            dxd = dot(jnp.concatenate([mt, mt], axis=1), jnp.concatenate(dycat, axis=0)) + dstate
            xa = xa_s[j, rows, :]
            dtp = dtp_s[j, rows, :]
            dy = dyf_s[rows, :]
            tail = jnp.sum(xa * dtp * dstate, axis=0, keepdims=True) + ea_s[
                j, pl.ds(c * BLOCK + BLOCK - 1, 1), :
            ] * jnp.sum(dsf_s[rows, :] * sin_s[j, rows, :], axis=0, keepdims=True)
            q = dxd * xa
            r = dy * y_s[j, rows, :] - q * dtp
            r = jnp.concatenate(
                [
                    r[: BLOCK - ROWS],
                    r[BLOCK - ROWS :] + jnp.where(iota(0, (ROWS, LANES)) == ROWS - 1, tail, 0.0),
                ],
                axis=0,
            )
            acc_s[rows, :] = acc_s[rows, :] + dot(halves(r), place_r) + dot(q.astype(BF16), place_q)
            du_s[j, rows, :] = (dxd * dtp + skips * dy) * gx_s[j, rows, :]
        for peer in sp_peers:
            z_copy(peer, sp, j).start()
        return carry

    lax.fori_loop(0, pairs, middle, 0)

    acc_t = [acc_s[pl.ds(c * BLOCK, BLOCK), :].T for c in range(chunks)]
    dlogs = dot(
        halves(jnp.concatenate([t[0:ROWS] for t in acc_t], axis=0)), jnp.concatenate([tri, tri], axis=0)
    )
    ga = jnp.zeros((ROWS, LANES), F32)
    for c in range(chunks):
        rows = pl.ds(c * BLOCK, BLOCK)
        dlog = dlogs[c * ROWS : (c + 1) * ROWS]
        ddt = acc_t[c][LANES // 2 : LANES // 2 + ROWS] - dlog * decay
        dd_s[c] = (ddt * sig_s[:, rows]).astype(BF16)
        ga = ga + dlog * step_s[:, rows]
    for peer in sp_peers:
        d_copy(peer, sp).start()
    ga_col = jnp.sum(ga, axis=1, keepdims=True)

    def ga_row(col):
        diag = iota(0, (ROWS, heads)) == iota(1, (ROWS, heads))
        return jnp.sum(jnp.where(diag, jnp.broadcast_to(col, (ROWS, heads)), 0.0), axis=0, keepdims=True)

    def ga_copy(peer, recv):
        return remote(ga_s, rga.at[recv], ga_send.at[peer], ga_recv.at[recv], "dp", peer)

    if reduce_here:
        ga_s[...] = jnp.broadcast_to(ga_col, ga_s.shape)
        for peer in dp_peers:
            ga_copy(peer, dp).start()
    else:
        oga_ref[...] = ga_row(ga_col)

    def convolve(i, carry):
        c = chunks - 1 - i
        base = pl.multiple_of(c * BLOCK, BLOCK)
        rows = pl.ds(base, BLOCK)
        for j in range(pairs):
            cols = pl.ds(j * LANES, LANES)
            dx_s[j, rows, :] = conv_back(du_s.at[j], base, tapx_v[:, cols].astype(F32)).astype(BF16)
        return carry

    lax.fori_loop(0, chunks, convolve, 0)
    for j in range(pairs):
        for peer in sp_peers:
            x_copy(peer, sp, j).start()

    def backward(i, carry):
        c = chunks - 1 - i
        base = pl.multiple_of(c * BLOCK, BLOCK)
        rows = pl.ds(base, BLOCK)
        dscores = jnp.zeros((BLOCK, BLOCK), F32)
        dcc = jnp.zeros((BLOCK, STATE), F32)
        dbb = jnp.zeros((BLOCK, STATE), F32)
        for j in range(pairs):
            cols = pl.ds(j * LANES, LANES)
            xdb = xdb_s[j, rows, :]
            xcat = jnp.concatenate([xdb * h for h in half_b], axis=0)
            dm = dot(dy_s[j, rows, :], jnp.concatenate([xcat, xcat], axis=1), ROWS_ROWS) * lam_s[j, rows, :]
            for k in range(per):
                dscores = dscores + dm[:, k * BLOCK : (k + 1) * BLOCK]

        def joined(ref):
            return jnp.concatenate([ref[j, rows, :].astype(BF16) for j in range(pairs)], axis=1)

        dcc = dot(joined(edy_s), joined(sin_s), ROWS_ROWS)
        dbb = dot(joined(xdte_s), joined(ds_s), ROWS_ROWS)
        dcc = dcc + dot(dscores.astype(BF16), bb_s[rows, :])
        dbb = dbb + dot(dscores.T.astype(BF16), cb_s[rows, :])
        dbu_s[rows, :] = dbb * gb_s[rows, :]
        dcu_s[rows, :] = dcc * gc_s[rows, :]
        dbc_s[rows, 0:STATE] = conv_back(dbu_s, base, tapb_v[:, gcols].astype(F32)).astype(BF16)
        dbc_s[rows, STATE : 2 * STATE] = conv_back(dcu_s, base, tapc_v[:, gcols].astype(F32)).astype(BF16)
        return carry

    mid = chunks // 2
    lax.fori_loop(0, mid, backward, 0)

    rd[sp] = dd_s[sp]
    for peer in sp_peers:
        d_copy(peer, peer).wait_recv()
    whole_d = jnp.concatenate([rd[k].astype(F32)[:heads] for k in range(n_sp)], axis=0).astype(BF16)
    od_ref[...] = whole_d
    arrived("li")
    whole_w = dot(whole_d, li_v[...])

    if reduce_here:
        width = part.shape[1] // n_dp

        def w1_copy(peer, recv):
            return remote(
                part.at[:, block(peer, width)], rs1.at[recv], w1_send.at[peer], w1_recv.at[recv], "dp", peer
            )

        def w2_copy(peer, recv):
            return remote(mine1, rs2.at[recv], w2_send.at[peer], w2_recv.at[recv], "sp", peer)

        def w3_copy(peer, recv):
            return remote(mine2, rs3.at[recv], w3_send.at[peer], w3_recv.at[recv], "dp", peer)

        part[...] = whole_w.astype(BF16)
        for peer in dp_peers:
            w1_copy(peer, dp).start()
        rs1[dp] = part[:, block(dp, width)]
    else:
        ow_ref[...] = whole_w

    lax.fori_loop(mid, chunks, backward, 0)

    if reduce_here:
        for peer in dp_peers:
            w1_copy(peer, peer).wait_recv()
        mine1[...] = add_all([rs1[k].astype(F32) for k in range(n_dp)]).astype(BF16)
        for peer in sp_peers:
            w2_copy(peer, sp).start()
        for peer in sp_peers:
            bc_copy(peer, sp).start()
        rs2[sp] = mine1[...]
        rga[dp] = ga_s[...]
        for peer in dp_peers:
            ga_copy(peer, peer).wait_recv()
        oga_ref[...] = ga_row(add_all([rga[k] for k in range(n_dp)])[:, 0:1])
        for peer in sp_peers:
            w2_copy(peer, peer).wait_recv()
        mine2[...] = add_all([rs2[k].astype(F32) for k in range(n_sp)]).astype(BF16)
        for peer in dp_peers:
            w3_copy(peer, dp).start()
        rs3[dp] = mine2[...]

    else:
        for peer in sp_peers:
            bc_copy(peer, sp).start()
    for j in range(pairs):
        oz_ref[:, block(sp * pairs + j, LANES)] = dz_s[j, ours, :]
        ox_ref[:, block(sp * pairs + j, LANES)] = dx_s[j, ours, :]
    rbc[sp] = dbc_s[ours, :]
    for peer in sp_peers:
        bc_copy(peer, peer).wait_recv()
    for g in range(GROUPS):
        total = add_all([rbc[g * group_span + k].astype(F32) for k in range(group_span)]).astype(BF16)
        ob_ref[:, g * STATE : (g + 1) * STATE] = total[:, 0:STATE]
        oc_ref[:, g * STATE : (g + 1) * STATE] = total[:, STATE : 2 * STATE]
    for peer in sp_peers:
        for j in range(pairs):
            z_copy(peer, peer, j).wait_recv()
            x_copy(peer, peer, j).wait_recv()
    if reduce_here:
        for peer in dp_peers:
            w3_copy(peer, peer).wait_recv()
        for k in range(n_dp):
            ow_ref[:, k * width : (k + 1) * width] = rs3[k].astype(F32)
    for peer in sp_peers:
        for copy in (bc_copy, d_copy):
            copy(peer, sp).wait_send()
        for j in range(pairs):
            cot_copy(peer, sp, j).wait_send()
            z_copy(peer, sp, j).wait_send()
            x_copy(peer, sp, j).wait_send()
        if reduce_here:
            w2_copy(peer, sp).wait_send()
    for peer in dp_peers:
        for copy in (ga_copy, w1_copy, w3_copy):
            copy(peer, dp).wait_send()


def fused(args, n_sp, n_dp, group_span, head_dim, heads, reduce_here):
    cot, li, x, z, b, c, dt, tapx, tapb, tapc, bias, alog, skip, nw = args
    length, channels = x.shape
    tokens, width = li.shape
    all_heads = heads * n_sp
    per = LANES // head_dim
    pairs = channels // LANES
    vm = pltpu.VMEM
    dma = pltpu.SemaphoreType.DMA
    wide = vm((pairs, length, LANES), F32)
    wide_b = vm((pairs, length, LANES), BF16)
    thin = vm((length, LANES), F32)
    thin_b = vm((length, LANES), BF16)
    padded = vm((length + PAD, LANES), F32)
    tall = vm((pairs, length + PAD, LANES), F32)
    rows = vm((ROWS, length), F32)
    piece = width // n_dp if reduce_here else LANES
    return pl.pallas_call(
        functools.partial(step_kernel, n_sp, n_dp, group_span, head_dim, heads, reduce_here),
        out_shape=(
            jax.ShapeDtypeStruct((tokens, channels * n_sp), BF16),
            jax.ShapeDtypeStruct((tokens, channels * n_sp), BF16),
            jax.ShapeDtypeStruct((tokens, GROUPS * STATE), BF16),
            jax.ShapeDtypeStruct((tokens, GROUPS * STATE), BF16),
            jax.ShapeDtypeStruct((all_heads, tokens), BF16),
            jax.ShapeDtypeStruct((1, heads), F32),
            jax.ShapeDtypeStruct((all_heads, width), F32),
        ),
        in_specs=[pl.BlockSpec(memory_space=pltpu.MemorySpace.HBM)] * 14,
        out_specs=tuple([pl.BlockSpec(memory_space=pltpu.VMEM)] * 7),
        scratch_shapes=[
            vm((tokens, channels * n_sp), BF16),
            vm((tokens, width), BF16),
            wide_b,
            wide_b,
            thin_b,
            thin_b,
            vm((heads, length), BF16),
            vm(tapx.shape, BF16),
            vm(tapb.shape, BF16),
            vm(tapc.shape, BF16),
            vm((1, heads), F32),
            vm((1, heads), F32),
            vm((1, heads), F32),
            vm((1, channels), F32),
            wide_b,
            tall,
            padded,
            padded,
            wide,
            wide,
            wide,
            wide,
            wide,
            wide,
            wide,
            wide_b,
            vm((pairs, STATE, LANES), F32),
            vm((pairs, length, per * BLOCK), F32),
            vm((pairs, length, per * BLOCK), BF16),
            wide_b,
            wide_b,
            vm((pairs, length, 2 * LANES), BF16),
            wide_b,
            tall,
            thin_b,
            thin_b,
            thin,
            thin,
            thin_b,
            padded,
            padded,
            vm((ROWS, channels), F32),
            rows,
            rows,
            vm((length // BLOCK * ROWS, LANES), F32),
            rows,
            vm((ROWS, LANES), F32),
            thin,
            thin,
            thin,
            wide_b,
            wide_b,
            vm((length, 2 * STATE), BF16),
            vm((length // BLOCK, ROWS, BLOCK), BF16),
            vm((n_sp, tokens, 2 * STATE), BF16),
            vm((n_sp, ROWS, BLOCK), BF16),
            vm((n_dp, ROWS, LANES), F32),
            vm((all_heads, width), BF16),
            vm((n_dp, all_heads, piece), BF16),
            vm((all_heads, piece), BF16),
            vm((n_sp, all_heads, piece), BF16),
            vm((all_heads, piece), BF16),
            vm((n_dp, all_heads, piece), BF16),
            dma((12 + 2 * pairs,)),
        ]
        + [dma((n_sp, pairs))] * 6
        + [dma((n_sp,))] * 4
        + [dma((n_dp,))] * 4
        + [dma((n_sp,))] * 2
        + [dma((n_dp,))] * 2,
        compiler_params=pltpu.CompilerParams(
            collective_id=0, has_side_effects=True, vmem_limit_bytes=40 * 1024 * 1024
        ),
    )(*args)


def out_kernel(count, *refs):
    srcs, dsts, sem = refs[:count], refs[count : 2 * count], refs[2 * count]
    copies = [pltpu.make_async_copy(s, d, sem.at[k]) for k, (s, d) in enumerate(zip(srcs, dsts))]
    for copy in copies:
        copy.start()
    for copy in copies:
        copy.wait()


def copy_out(arrays):
    n = len(arrays)
    return pl.pallas_call(
        functools.partial(out_kernel, n),
        out_shape=tuple(jax.ShapeDtypeStruct(a.shape, a.dtype) for a in arrays),
        in_specs=[pl.BlockSpec(memory_space=pltpu.VMEM)] * n,
        out_specs=tuple([pl.BlockSpec(memory_space=pltpu.MemorySpace.HBM)] * n),
        scratch_shapes=[pltpu.SemaphoreType.DMA((n,))],
        compiler_params=pltpu.CompilerParams(vmem_limit_bytes=1024 * 1024),
    )(*arrays)


def shards(
    cotangent,
    layer_input,
    x_pre,
    z_pre,
    b_pre,
    c_pre,
    dt_raw,
    conv_x,
    conv_b,
    conv_c,
    dt_bias,
    a_log,
    d_skip,
    norm_w,
):
    n_sp = lax.axis_size("sp")
    n_dp = lax.axis_size("dp")
    assert x_pre.shape[0] == 1
    assert cotangent.shape[1] == BLOCK
    heads_here = dt_raw.shape[2]
    heads = heads_here * n_sp
    head_dim = x_pre.shape[2] // heads_here
    group_span = n_sp // GROUPS
    reduce_here = heads % 16 == 0 and (layer_input.shape[2] // n_dp) % LANES == 0
    args = (
        cotangent[0],
        layer_input[0],
        x_pre[0],
        z_pre[0],
        b_pre[0],
        c_pre[0],
        dt_raw[0].T,
        conv_x,
        conv_b,
        conv_c,
        dt_bias[None],
        a_log[None],
        d_skip[None],
        norm_w[None],
    )
    args = tuple(pltpu.with_memory_space_constraint(a, pltpu.MemorySpace.HBM) for a in args)
    ox, oz, ob, oc, od, oga, ow = copy_out(
        fused(args, n_sp, n_dp, group_span, head_dim, heads_here, reduce_here)
    )
    grad_a_log = oga[0]
    if not reduce_here:
        ow, grad_a_log = lax.psum((ow, grad_a_log), "dp")
        ow = lax.psum(ow, "sp")
    return ox[None], oz[None], ob[None], oc[None], od.T[None], grad_a_log, ow.T


def solution(mesh):
    placed = (
        P("dp", "sp", None),
        P("dp", "sp", None),
        P("dp", None, "sp"),
        P("dp", None, "sp"),
        P("dp", None, None),
        P("dp", None, None),
        P("dp", None, "sp"),
        P(None, "sp"),
        P(),
        P(),
        P("sp"),
        P("sp"),
        P("sp"),
        P("sp"),
    )
    return jax.shard_map(
        shards,
        mesh=mesh,
        in_specs=placed,
        out_specs=(
            P("dp", "sp", None),
            P("dp", "sp", None),
            P("dp", "sp", None),
            P("dp", "sp", None),
            P("dp", "sp", None),
            P("sp"),
            P(),
        ),
        check_vma=False,
    )
```

time: 58.9 us -> 36.2 us (0.61)
  Pallas kernels: 48.8 us -> 35.3 us
  local copies, waits for them, and re-layouts: 9.01 us -> 0 us
    pallas_call x3 -> x2, Pallas kernels: 48.8 us -> 35.3 us  [the longest x1 34.2 us: fused(): pl.pallas_call(functools.partial(step_kernel, n_sp, n_dp, group_span, hea...]
    unnamed x35 -> x0, local copies, waits for them, and re-layouts: 8.31 us -> none
where the time goes in v1:
time: 36.2 us; the launch traced here: 36 us
  Pallas kernels  35.3 us (98%)
  between operations  0.65 us (2%)
    pallas_call x1, Pallas kernels, fused(): pl.pallas_call(functools.partial(step_kernel, n_sp, n_dp, group_span, hea...  34.2 us
    pallas_call x1, Pallas kernels, copy_out(): pl.pallas_call(functools.partial(out_kernel, n), out_shape=tuple((jax.Sha...  1.16 us

profile of v1, /device:TPU:0, one launch (start us, length us, event | category | flops | bytes accessed | tf_op | source)
XLA Modules:
  0.0 36.0 jit_solution(6069602674547858797)
XLA Ops:
  0.6 34.2 %shard_map.189 = (bf16[128,2048]{1,0:T(8,128)(2,1)S(1)}, bf16[128,2048]{1,0:T(8,128)(2,1)S(1)}, bf16[128,256]{1,0:T(8,128)(2,1)S(1)}, bf16[128,256]{1,0:T(8,128)...) custom-call(bf16[128,2048]{1,0:T(8,128)(2,1)} %bitcast.22, ...), custom_call_target="tpu_custom_call" | custom-call | tf_op jit(solution)/shard_map/pallas_call | solution.py:647
  34.8 1.2 %shard_map.190 = (bf16[128,2048]{1,0:T(8,128)(2,1)}, bf16[128,2048]{1,0:T(8,128)(2,1)}, bf16[128,256]{1,0:T(8,128)(2,1)}, bf16[128,256]{1,0:T(8,128)(2,1)}, bf16...) custom-call(bf16[128,2048]{1,0:T(8,128)(2,1)S(1)} %get-tuple-element.21.refs_0_, ...), custom_call_target="tpu_custom_call" | custom-call | tf_op jit(solution)/shard_map/pallas_call | solution.py:748

commit v2 on v1

--- a/solution.py
+++ b/solution.py
@@ -125,6 +125,7 @@
     acc_s,
     dyf_s,
     dsf_s,
+    edyl_s,
     dz_s,
     dx_s,
     dbc_s,
@@ -360,7 +361,7 @@
                 his.append(hi)
                 los.append((m - hi.astype(F32)).astype(BF16))
                 lam_s[j, rows, k * BLOCK : (k + 1) * BLOCK] = lam
-                m_s[j, rows, k * BLOCK : (k + 1) * BLOCK] = hi
+                m_s[j, rows, k * BLOCK : (k + 1) * BLOCK] = m
             ap = pick(acols)
             dtp = pick(dcols)
             dtp_s[j, rows, :] = dtp
@@ -398,6 +399,12 @@
         cols = block(j, LANES)
         for peer in sp_peers:
             cot_copy(peer, peer, j).wait_recv()
+
+        @pl.when(j > 0)
+        def _():
+            for peer in sp_peers:
+                z_copy(peer, sp, j - 1).start()
+
         gain = cp_s[0:1, cols]
         skips = cp_s[1:2, cols]
         place_r = jnp.where(row // head_dim + j * per == lane, 1.0, 0.0).astype(BF16)
@@ -425,24 +432,36 @@
                 dy = dgated * sz
                 dyf_s[rows, :] = dy
                 dy_s[j, rows, :] = halves(dy)
-                edy_s[j, rows, :] = (ea_s[j, rows, :] * dy).astype(BF16)
+                edy = ea_s[j, rows, :] * dy
+                edy_hi = edy.astype(BF16)
+                edy_s[j, rows, :] = edy_hi
+                edyl_s[rows, :] = (edy - edy_hi.astype(F32)).astype(BF16)
         ds = jnp.zeros((STATE, LANES), F32)
         for c in reversed(range(chunks)):
             rows = pl.ds(c * BLOCK, BLOCK)
             dsf_s[rows, :] = ds
-            ds_s[j, rows, :] = ds.astype(BF16)
+            ds_hi = ds.astype(BF16)
+            ds_s[j, rows, :] = ds_hi
             if c > 0:
                 last = pl.ds(c * BLOCK + BLOCK - 1, 1)
-                ds = ds * ea_s[j, last, :] + dot(ct_s[rows, :], edy_s[j, rows, :])
+                ct = ct_s[rows, :]
+                ds = ds * ea_s[j, last, :] + dot(
+                    jnp.concatenate([ct, ct], axis=1),
+                    jnp.concatenate([edy_s[j, rows, :], edyl_s[rows, :]], axis=0),
+                )
         for c in reversed(range(chunks)):
             rows = pl.ds(c * BLOCK, BLOCK)
             dy2 = dy_s[j, rows, :]
-            mt = jnp.concatenate(
-                [m_s[j, rows, k * BLOCK : (k + 1) * BLOCK].astype(F32).T.astype(BF16) for k in range(per)], axis=1
+            mt2 = halves(
+                jnp.concatenate([m_s[j, rows, k * BLOCK : (k + 1) * BLOCK].T for k in range(per)], axis=1)
             )
             dycat = [dy2[:, p * LANES : (p + 1) * LANES] * h for p in range(2) for h in half_b]
-            dstate = te_s[j, rows, :] * dot(bb_s[rows, :], ds_s[j, rows, :])
-            dxd = dot(jnp.concatenate([mt, mt], axis=1), jnp.concatenate(dycat, axis=0)) + dstate
+            bb = bb_s[rows, :]
+            dstate = te_s[j, rows, :] * dot(
+                bb, ds_s[j, rows, :]
+            )
+            mt3 = jnp.concatenate([mt2[:, : per * BLOCK], mt2], axis=1)
+            dxd = dot(mt3, jnp.concatenate(dycat[per:] + dycat[:per] + dycat[:per], axis=0)) + dstate
             xa = xa_s[j, rows, :]
             dtp = dtp_s[j, rows, :]
             dy = dyf_s[rows, :]
@@ -460,8 +479,6 @@
             )
             acc_s[rows, :] = acc_s[rows, :] + dot(halves(r), place_r) + dot(q.astype(BF16), place_q)
             du_s[j, rows, :] = (dxd * dtp + skips * dy) * gx_s[j, rows, :]
-        for peer in sp_peers:
-            z_copy(peer, sp, j).start()
         return carry
 
     lax.fori_loop(0, pairs, middle, 0)
@@ -479,6 +496,8 @@
         ga = ga + dlog * step_s[:, rows]
     for peer in sp_peers:
         d_copy(peer, sp).start()
+    for peer in sp_peers:
+        z_copy(peer, sp, pairs - 1).start()
     ga_col = jnp.sum(ga, axis=1, keepdims=True)
 
     def ga_row(col):
@@ -505,7 +524,8 @@
         return carry
 
     lax.fori_loop(0, chunks, convolve, 0)
-    for j in range(pairs):
+    early = pairs // 2 if reduce_here else pairs
+    for j in range(early):
         for peer in sp_peers:
             x_copy(peer, sp, j).start()
 
@@ -577,6 +597,9 @@
         mine1[...] = add_all([rs1[k].astype(F32) for k in range(n_dp)]).astype(BF16)
         for peer in sp_peers:
             w2_copy(peer, sp).start()
+        for j in range(early, pairs):
+            for peer in sp_peers:
+                x_copy(peer, sp, j).start()
         for peer in sp_peers:
             bc_copy(peer, sp).start()
         rs2[sp] = mine1[...]
@@ -599,32 +622,36 @@
         ox_ref[:, block(sp * pairs + j, LANES)] = dx_s[j, ours, :]
     rbc[sp] = dbc_s[ours, :]
     for peer in sp_peers:
+        d_copy(peer, sp).wait_send()
+        for j in range(pairs):
+            cot_copy(peer, sp, j).wait_send()
+            z_copy(peer, sp, j).wait_send()
+            z_copy(peer, peer, j).wait_recv()
+        for j in range(early):
+            x_copy(peer, peer, j).wait_recv()
+            x_copy(peer, sp, j).wait_send()
+    for peer in dp_peers:
+        ga_copy(peer, dp).wait_send()
+        w1_copy(peer, dp).wait_send()
+    for peer in sp_peers:
+        if reduce_here:
+            w2_copy(peer, sp).wait_send()
+        for j in range(early, pairs):
+            x_copy(peer, peer, j).wait_recv()
+            x_copy(peer, sp, j).wait_send()
+    for peer in sp_peers:
         bc_copy(peer, peer).wait_recv()
+        bc_copy(peer, sp).wait_send()
     for g in range(GROUPS):
         total = add_all([rbc[g * group_span + k].astype(F32) for k in range(group_span)]).astype(BF16)
         ob_ref[:, g * STATE : (g + 1) * STATE] = total[:, 0:STATE]
         oc_ref[:, g * STATE : (g + 1) * STATE] = total[:, STATE : 2 * STATE]
-    for peer in sp_peers:
-        for j in range(pairs):
-            z_copy(peer, peer, j).wait_recv()
-            x_copy(peer, peer, j).wait_recv()
     if reduce_here:
         for peer in dp_peers:
             w3_copy(peer, peer).wait_recv()
+            w3_copy(peer, dp).wait_send()
         for k in range(n_dp):
             ow_ref[:, k * width : (k + 1) * width] = rs3[k].astype(F32)
-    for peer in sp_peers:
-        for copy in (bc_copy, d_copy):
-            copy(peer, sp).wait_send()
-        for j in range(pairs):
-            cot_copy(peer, sp, j).wait_send()
-            z_copy(peer, sp, j).wait_send()
-            x_copy(peer, sp, j).wait_send()
-        if reduce_here:
-            w2_copy(peer, sp).wait_send()
-    for peer in dp_peers:
-        for copy in (ga_copy, w1_copy, w3_copy):
-            copy(peer, dp).wait_send()
 
 
 def fused(args, n_sp, n_dp, group_span, head_dim, heads, reduce_here):
@@ -686,7 +713,7 @@
             wide_b,
             vm((pairs, STATE, LANES), F32),
             vm((pairs, length, per * BLOCK), F32),
-            vm((pairs, length, per * BLOCK), BF16),
+            vm((pairs, length, per * BLOCK), F32),
             wide_b,
             wide_b,
             vm((pairs, length, 2 * LANES), BF16),
@@ -708,6 +735,7 @@
             thin,
             thin,
             thin,
+            thin_b,
             wide_b,
             wide_b,
             vm((length, 2 * STATE), BF16),

time: 36.2 us -> 35.3 us (0.975)
  Pallas kernels: 35.3 us -> 34.4 us
    pallas_call x1, Pallas kernels: 34.2 us -> 33.3 us  [fused(): pl.pallas_call(functools.partial(step_kernel, n_sp, n_dp, group_span, hea...]
where the time goes in v2:
time: 35.3 us; the launch traced here: 35.1 us
  Pallas kernels  34.4 us (97%)
  between operations  0.65 us (2%)
    pallas_call x1, Pallas kernels, fused(): pl.pallas_call(functools.partial(step_kernel, n_sp, n_dp, group_span, hea...  33.3 us
    pallas_call x1, Pallas kernels, copy_out(): pl.pallas_call(functools.partial(out_kernel, n), out_shape=tuple((jax.Sha...  1.16 us

profile of v2, /device:TPU:0, one launch (start us, length us, event | category | flops | bytes accessed | tf_op | source)
XLA Modules:
  0.0 35.1 jit_solution(1081396271117154160)
XLA Ops:
  0.6 33.3 %shard_map.189 = (bf16[128,2048]{1,0:T(8,128)(2,1)S(1)}, bf16[128,2048]{1,0:T(8,128)(2,1)S(1)}, bf16[128,256]{1,0:T(8,128)(2,1)S(1)}, bf16[128,256]{1,0:T(8,128)...) custom-call(bf16[128,2048]{1,0:T(8,128)(2,1)} %bitcast.22, ...), custom_call_target="tpu_custom_call" | custom-call | tf_op jit(solution)/shard_map/pallas_call | solution.py:674
  33.9 1.2 %shard_map.190 = (bf16[128,2048]{1,0:T(8,128)(2,1)}, bf16[128,2048]{1,0:T(8,128)(2,1)}, bf16[128,256]{1,0:T(8,128)(2,1)}, bf16[128,256]{1,0:T(8,128)(2,1)}, bf16...) custom-call(bf16[128,2048]{1,0:T(8,128)(2,1)S(1)} %get-tuple-element.21.refs_0_, ...), custom_call_target="tpu_custom_call" | custom-call | tf_op jit(solution)/shard_map/pallas_call | solution.py:776

commit v3 on v2

--- a/solution.py
+++ b/solution.py
@@ -523,12 +523,6 @@
             dx_s[j, rows, :] = conv_back(du_s.at[j], base, tapx_v[:, cols].astype(F32)).astype(BF16)
         return carry
 
-    lax.fori_loop(0, chunks, convolve, 0)
-    early = pairs // 2 if reduce_here else pairs
-    for j in range(early):
-        for peer in sp_peers:
-            x_copy(peer, sp, j).start()
-
     def backward(i, carry):
         c = chunks - 1 - i
         base = pl.multiple_of(c * BLOCK, BLOCK)
@@ -588,6 +582,12 @@
         rs1[dp] = part[:, block(dp, width)]
     else:
         ow_ref[...] = whole_w
+
+    lax.fori_loop(0, chunks, convolve, 0)
+    early = pairs // 2 if reduce_here else pairs
+    for j in range(early):
+        for peer in sp_peers:
+            x_copy(peer, sp, j).start()
 
     lax.fori_loop(mid, chunks, backward, 0)
 

time: 35.3 us -> 35.3 us (level)
  no operation moved by 1% of the time
where the time goes in v3:
time: 35.3 us; the launch traced here: 35.1 us
  Pallas kernels  34.4 us (97%)
  between operations  0.65 us (2%)
    pallas_call x1, Pallas kernels, fused(): pl.pallas_call(functools.partial(step_kernel, n_sp, n_dp, group_span, hea...  33.3 us
    pallas_call x1, Pallas kernels, copy_out(): pl.pallas_call(functools.partial(out_kernel, n), out_shape=tuple((jax.Sha...  1.16 us

profile of v3, /device:TPU:0, one launch (start us, length us, event | category | flops | bytes accessed | tf_op | source)
XLA Modules:
  0.0 35.1 jit_solution(1331186388249491442)
XLA Ops:
  0.6 33.3 %shard_map.189 = (bf16[128,2048]{1,0:T(8,128)(2,1)S(1)}, bf16[128,2048]{1,0:T(8,128)(2,1)S(1)}, bf16[128,256]{1,0:T(8,128)(2,1)S(1)}, bf16[128,256]{1,0:T(8,128)...) custom-call(bf16[128,2048]{1,0:T(8,128)(2,1)} %bitcast.22, ...), custom_call_target="tpu_custom_call" | custom-call | tf_op jit(solution)/shard_map/pallas_call | solution.py:674
  33.9 1.2 %shard_map.190 = (bf16[128,2048]{1,0:T(8,128)(2,1)}, bf16[128,2048]{1,0:T(8,128)(2,1)}, bf16[128,256]{1,0:T(8,128)(2,1)}, bf16[128,256]{1,0:T(8,128)(2,1)}, bf16...) custom-call(bf16[128,2048]{1,0:T(8,128)(2,1)S(1)} %get-tuple-element.21.refs_0_, ...), custom_call_target="tpu_custom_call" | custom-call | tf_op jit(solution)/shard_map/pallas_call | solution.py:776
